TPU v7x, 32 devices: a whole 2x2x4 slice. The times are simulated.
32 devices in a mesh: sp: 8 (over z, x), tp: 4 (over y, core).
Axes of the slice: x: 2, y: 2, z: 4, core: 2. Of those that a mesh axis runs over, the one named last changes fastest.
Arguments:
- layer_input: bfloat16 [8, 4096, 2048], P(None, ('sp', 'tp')), may hold values from -6 to 6
- norm_gain: bfloat16 [2048], replicated, may hold values from 0.099609375 to 1.8984375
- key_weight: bfloat16 [2048, 1024], replicated, may hold values from -0.125 to 0.125
- value_weight: bfloat16 [2048, 1024], replicated, may hold values from -0.125 to 0.125
- new_query: bfloat16 [8, 1024], P('sp', 'tp'), may hold values from -12 to 12
- score_offset: float32 [8], replicated, may hold values from -10 to -3.5
Outputs:
- key_cache: bfloat16 [8, 4096, 1024], P('sp', None, 'tp')
- value_cache: bfloat16 [8, 4096, 1024], P('sp', None, 'tp')
- first_read: float32 [8, 1024], P('sp', 'tp')
All inputs are finite; a program needn't handle non-finite values.
Results may differ from a plain program's by a relative error of at most 0.0082.
Values may be sent and summed in bfloat16 or wider, within the bound.
A program may use at most 128 MiB of HBM per device.

v0:
```python
import jax
import jax.numpy as jnp
from jax import lax
from jax.sharding import PartitionSpec as P

norm_epsilon = 1e-06


def shards(layer_input, norm_gain, key_weight, value_weight, new_query, score_offset):
    seq_count, positions, model_width = layer_input.shape
    groups = lax.axis_size("tp")
    head_count = score_offset.shape[0]
    local_heads = head_count // groups
    head_dim = new_query.shape[1] // local_heads
    columns = local_heads * head_dim
    score_scale = head_dim ** (-0.5)
    wide = layer_input.astype(jnp.float32)
    normed = (
        wide
        * lax.rsqrt(jnp.mean(wide * wide, axis=-1, keepdims=True) + norm_epsilon)
        * norm_gain.astype(jnp.float32)
    ).astype(jnp.bfloat16)
    key_split = key_weight.reshape(model_width, groups, columns)
    value_split = value_weight.reshape(model_width, groups, columns)
    keys = jnp.einsum(
        "spd,dtc->stpc", normed, key_split, preferred_element_type=jnp.float32
    ).astype(jnp.bfloat16)
    values = jnp.einsum(
        "spd,dtc->stpc", normed, value_split, preferred_element_type=jnp.float32
    ).astype(jnp.bfloat16)
    stacked = jnp.stack((keys, values), axis=2)
    direct = stacked.reshape(seq_count * groups, 2, positions, columns)
    received = lax.all_to_all(direct, ("sp", "tp"), split_axis=0, concat_axis=2, tiled=True)
    arrived = received.reshape(2, -1, columns)
    key_cache = arrived[0][None]
    value_cache = arrived[1][None]
    own_keys = arrived[0].reshape(-1, local_heads, head_dim)
    own_values = arrived[1].reshape(-1, local_heads, head_dim)
    own_offsets = lax.dynamic_slice_in_dim(
        score_offset, lax.axis_index("tp") * local_heads, local_heads
    )
    query_own = new_query.reshape(local_heads, head_dim)
    scores = jnp.einsum("hd,phd->hp", query_own, own_keys, preferred_element_type=jnp.float32)
    scores = scores * score_scale + own_offsets[:, None]
    log_rest = jax.nn.log_sigmoid(-scores)
    later = lax.cumsum(log_rest, axis=1, reverse=True) - log_rest
    weights = jnp.exp(jax.nn.log_sigmoid(scores) + later).astype(jnp.bfloat16)
    reading = jnp.einsum("hp,phd->hd", weights, own_values, preferred_element_type=jnp.float32)
    first_read = reading * lax.rsqrt(
        jnp.mean(reading * reading, axis=-1, keepdims=True) + norm_epsilon
    )
    return (key_cache, value_cache, first_read.reshape(1, columns))


def solution(mesh):
    placed = (P(None, ("sp", "tp"), None), P(), P(), P(), P("sp", "tp"), P())
    return jax.shard_map(
        shards,
        mesh=mesh,
        in_specs=placed,
        out_specs=(P("sp", None, "tp"), P("sp", None, "tp"), P("sp", "tp")),
        check_vma=False,
    )
```

profile of v0, /device:TPU:0, one launch (start us, length us, event | category | flops | bytes accessed | tf_op | source)
XLA Modules:
  0.0 139.0 jit_solution(2495934026409444317)
XLA Ops:
  0.6 0.0 copy-start
  0.6 0.0 copy-start.2
  0.7 0.0 copy-start.3
  0.7 3.2 %fusion = f32[8,128]{1,0:T(8,128)S(1)} fusion(bf16[8,128,2048]{2,1,0:T(8,128)(2,1)} %param.6), kind=kLoop, calls=%fused_computation.2 | loop fusion | flops 6290432 | bytes 4198400 | tf_op jit(solution)/shard_map/reduce_sum | solution.py:20
  3.9 0.0 copy-done.3
  3.9 0.2 copy-done.2
  4.1 0.0 copy-start.4
  4.1 7.2 %fusion.17 = bf16[8,128,4,256]{3,1,2,0:T(8,128)(2,1)S(1)} fusion(bf16[256,4,8,256]{3,2,1,0:T(8,128)(2,1)} %bitcast.94, bf16[8,128,2048]{2,1,0:T(8,128)(2,1)S(1)} %copy-done.2, f32[2048]{0:T(1024)S(1)} %convert_element_type.25, f32[8,128]{1,0:T(8,128)S(1)} %add_rsqrt_fusion), kind=kOutput, calls=%fused_computation.18 | convolution fusion | flops 4304404480 | bytes 10498048 | tf_op jit(solution)/shard_map/spd,dtc->stpc/dot_general | solution.py:28
  11.3 0.0 copy-done.4
  11.3 4.8 %fusion.14 = bf16[8,128,4,256]{3,1,2,0:T(8,128)(2,1)S(1)} fusion(bf16[256,4,8,256]{3,2,1,0:T(8,128)(2,1)S(1)} %bitcast.95, bf16[8,128,2048]{2,1,0:T(8,128)(2,1)S(1)} %copy-done.2, f32[2048]{0:T(1024)S(1)} %convert_element_type.25, f32[8,128]{1,0:T(8,128)S(1)} %add_rsqrt_fusion), kind=kOutput, calls=%fused_computation.17 | convolution fusion | flops 4304404480 | bytes 10498048 | tf_op jit(solution)/shard_map/spd,dtc->stpc/dot_general | solution.py:25
  16.2 2.3 %pad_maximum_fusion = bf16[32,2,128,256]{3,2,1,0:T(8,128)(2,1)} fusion(bf16[32,1,128,256]{3,2,1,0:T(8,128)(2,1)S(1)} %bitcast.88, bf16[32,1,128,256]{3,2,1,0:T(8,128)(2,1)S(1)} %bitcast.89), kind=kLoop, calls=%fused_computation.12 | loop fusion | flops 2097152 | bytes 8388608 | tf_op jit(solution)/shard_map/stack | solution.py:31
  18.5 0.0 copy-start.5
  18.5 7.5 %all-to-all-start = ((bf16[32,2,128,256]{3,2,1,0:T(8,128)(2,1)}), bf16[32,2,128,256]{3,2,1,0:T(8,128)(2,1)}, u32[]{:S(2)}, u32[]{:S(2)}) async-start(bf16[32,2,128,256]{3,2,1,0:T(8,128)(2,1)} %pad_maximum_fusion), calls=%async_computation | async-start | bytes 8388608 | tf_op jit(solution)/shard_map/all_to_all | solution.py:33
  26.0 0.0 copy-done.5
  26.0 0.1 dynamic_slice.3
  26.1 94.1 %all-to-all-done = bf16[32,2,128,256]{3,2,1,0:T(8,128)(2,1)} async-done(((bf16[32,2,128,256]{3,2,1,0:T(8,128)(2,1)}), bf16[32,2,128,256]{3,2,1,0:T(8,128)(2,1)}, u32[]{:S(2)}, u32[]{:S(2)}) %all-to-all-start) | async-done | bytes 4194336 | tf_op jit(solution)/shard_map/all_to_all | solution.py:33
  120.2 3.9 %fusion.30 = (bf16[1,1,32,128,256]{4,3,1,2,0:T(8,128)(2,1)S(1)}, bf16[1,1,32,128,256]{4,3,1,2,0:T(8,128)(2,1)}) fusion(bf16[1,2,32,128,256]{4,3,1,2,0:T(8,128)(2,1)} %bitcast.12), kind=kLoop, calls=%fused_computation.40 | loop fusion | bytes 8388608 | tf_op jit(solution)/shard_map/slice | solution.py:36
  124.2 4.3 %reshape_squeeze.6 = bf16[4096,2,128]{2,1,0:T(2,128)(2,1)} reshape(bf16[1,1,32,128,256]{4,3,1,2,0:T(8,128)(2,1)} %get-tuple-element.4) | data formatting | bytes 4194304 | tf_op jit(solution)/shard_map/reshape;squeeze | solution.py:37
  128.5 0.0 copy-done
  128.5 2.2 %fusion.12 = f32[2,1,4096]{2,1,0:T(1,128)S(1)} fusion(bf16[4096,2,128]{2,1,0:T(2,128)(2,1)} %reshape_squeeze.6, bf16[1,256]{1,0:T(2,128)(2,1)S(1)} %copy-done), kind=kOutput, calls=%fused_computation.15 | convolution fusion | flops 2097152 | bytes 2130432 | tf_op jit(solution)/shard_map/hd,phd->hp/dot_general | solution.py:43
  130.7 0.2 fusion.29
  130.9 2.5 %reduce-window.6 = f32[2,32,128]{2,1,0:T(8,128)S(1)} reduce-window(f32[2,32,128]{2,1,0:T(8,128)S(1)} %bitcast.90, f32[]{:T(128)} %constant.9.clone.1), window={size=1x1x128 pad=0_0x0_0x0_127}, to_apply=%region_1.2 | reduce-window | flops 1040384 | bytes 65540 | tf_op jit(solution)/shard_map/reduce-window
  133.4 0.1 slice_reduce_fusion
  133.5 0.3 reduce-window.9
  133.8 0.1 slice.25
  133.8 0.1 add_bitcast_fusion
  133.9 0.3 fusion.27
  134.2 2.1 %reshape_squeeze.7 = bf16[4096,2,128]{2,1,0:T(2,128)(2,1)} reshape(bf16[1,1,32,128,256]{4,3,1,2,0:T(8,128)(2,1)S(1)} %get-tuple-element.3) | data formatting | bytes 4194304 | tf_op jit(solution)/shard_map/reshape;squeeze | solution.py:38
  136.3 0.0 copy-done.1
  136.3 2.0 %fusion.10 = f32[2,1,128]{2,1,0:T(1,128)S(1)} fusion(bf16[4096,2,128]{2,1,0:T(2,128)(2,1)} %reshape_squeeze.7, bf16[2,4096,1]{1,0,2:T(2,128)(2,1)S(1)} %fusion.27), kind=kOutput, calls=%fused_computation.13 | convolution fusion | flops 2097152 | bytes 2114560 | tf_op jit(solution)/shard_map/hp,phd->hd/dot_general | solution.py:48
  138.3 0.1 multiply_reduce_fusion
  138.4 0.6 broadcast_multiply_fusion
  (5 shorter events, 0.0 us)
Async XLA Ops:
  0.6 127.9 %copy-start = (bf16[1,256]{1,0:T(2,128)(2,1)S(1)}, bf16[1,256]{1,0:T(2,128)(2,1)}, u32[]{:S(2)}) copy-start(bf16[1,256]{1,0:T(2,128)(2,1)} %param.10) | copy-start | bytes 1540
  0.6 3.5 %copy-start.2 = (bf16[8,128,2048]{2,1,0:T(8,128)(2,1)S(1)}, bf16[8,128,2048]{2,1,0:T(8,128)(2,1)}, u32[]{:S(2)}) copy-start(bf16[8,128,2048]{2,1,0:T(8,128)(2,1)} %param.6) | copy-start | bytes 12582916
  0.7 3.3 %copy-start.3 = (bf16[2048]{0:T(1024)(128)(2,1)S(1)}, bf16[2048]{0:T(1024)(128)(2,1)}, u32[]{:S(2)}) copy-start(bf16[2048]{0:T(1024)(128)(2,1)} %param.7) | copy-start | bytes 12292
  4.1 7.2 %copy-start.4 = (bf16[2048,1024]{1,0:T(8,128)(2,1)S(1)}, bf16[2048,1024]{1,0:T(8,128)(2,1)}, u32[]{:S(2)}) copy-start(bf16[2048,1024]{1,0:T(8,128)(2,1)} %param.8) | copy-start | bytes 12582916
  18.5 7.5 %copy-start.5 = (f32[8]{0:T(128)S(1)}, f32[8]{0:T(128)}, u32[]{:S(2)}) copy-start(f32[8]{0:T(128)} %param.11) | copy-start | bytes 100
  18.5 101.7 %all-to-all-start = ((bf16[32,2,128,256]{3,2,1,0:T(8,128)(2,1)}), bf16[32,2,128,256]{3,2,1,0:T(8,128)(2,1)}, u32[]{:S(2)}, u32[]{:S(2)}) async-start(bf16[32,2,128,256]{3,2,1,0:T(8,128)(2,1)} %pad_maximum_fusion), calls=%async_computation | async-start | bytes 8388608 | tf_op jit(solution)/shard_map/all_to_all | solution.py:33
  124.2 12.1 %copy-start.1 = (bf16[1,1,32,128,256]{4,3,1,2,0:T(8,128)(2,1)}, bf16[1,1,32,128,256]{4,3,1,2,0:T(8,128)(2,1)S(1)}, u32[]{:S(2)}) copy-start(bf16[1,1,32,128,256]{4,3,1,2,0:T(8,128)(2,1)S(1)} %get-tuple-element.3) | copy-start | bytes 6291460
where the time goes:
time: 139 us
  waiting for transfers between devices  94.1 us (68%)
  matrix products  16.2 us (12%)
  local copies, waits for them, and re-layouts  10.8 us (8%)
  other arithmetic  9.61 us (7%)
  starting transfers between devices  7.46 us (5%)
    all_to_all x1, waiting for transfers between devices, shards(): lax.all_to_all(direct, ('sp', 'tp'), split_axis=0, concat_axis=2, tiled=T...  94.1 us
    all_to_all x1, starting transfers between devices, shards(): lax.all_to_all(direct, ('sp', 'tp'), split_axis=0, concat_axis=2, tiled=T...  7.46 us
    dot_general x1, matrix products, shards(): jnp.einsum('spd,dtc->stpc', normed, value_split, preferred_element_type=j...  7.19 us
    dot_general x1, matrix products, shards(): jnp.einsum('spd,dtc->stpc', normed, key_split, preferred_element_type=jnp...  4.84 us
    another operation x1, local copies, waits for them, and re-layouts, shards(): own_keys = arrived[0].reshape(-1, local_heads, head_dim)  4.32 us
    slice x1, local copies, waits for them, and re-layouts, shards(): value_cache = arrived[1][None]  3.93 us
    reduce_sum x1, other arithmetic, shards(): jnp.mean(wide * wide, axis=-1, keepdims=True) + norm_epsilon  3.23 us
  transfers between devices with their start and end apart: 1, of which 1 were waited for; matrix products, arithmetic and copies ran while one was open for 0% of the time, Pallas kernels for 0%

commit v1 on v0

--- a/solution.py
+++ b/solution.py
@@ -30,7 +30,12 @@
     ).astype(jnp.bfloat16)
     stacked = jnp.stack((keys, values), axis=2)
     direct = stacked.reshape(seq_count * groups, 2, positions, columns)
-    received = lax.all_to_all(direct, ("sp", "tp"), split_axis=0, concat_axis=2, tiled=True)
+    received = jnp.concatenate(
+        lax.all_to_all(
+            jnp.stack(jnp.split(direct, lax.axis_size(("sp", "tp")), axis=0)), ("sp", "tp"), 0, 0
+        ),
+        axis=2,
+    )
     arrived = received.reshape(2, -1, columns)
     key_cache = arrived[0][None]
     value_cache = arrived[1][None]

time: 139 us -> 158 us (1.14)
  other arithmetic: 9.61 us -> 28.3 us
    unnamed x2 -> x33, other arithmetic: 0.24 us -> 20.6 us
    dot_general x1, matrix products: 4.84 us -> 7.19 us  [shards(): jnp.einsum('spd,dtc->stpc', normed, key_split, preferred_element_type=jnp...]
    dot_general x1, matrix products: 7.19 us -> 4.84 us  [shards(): jnp.einsum('spd,dtc->stpc', normed, value_split, preferred_element_type=j...]
    another operation x3, other arithmetic: 5.09 us -> 3.44 us
where the time goes in v1:
time: 158 us
  waiting for transfers between devices  94.1 us (60%)
  other arithmetic  28.3 us (18%)
  matrix products  16.2 us (10%)
  local copies, waits for them, and re-layouts  10.8 us (7%)
  starting transfers between devices  7.46 us (5%)
    all_to_all x1, waiting for transfers between devices, shards(): lax.all_to_all(jnp.stack(jnp.split(direct, lax.axis_size(('sp', 'tp')), a...  94.1 us
    unnamed x33, other arithmetic  20.6 us
    all_to_all x1, starting transfers between devices, shards(): lax.all_to_all(jnp.stack(jnp.split(direct, lax.axis_size(('sp', 'tp')), a...  7.46 us
    dot_general x1, matrix products, shards(): jnp.einsum('spd,dtc->stpc', normed, key_split, preferred_element_type=jnp...  7.19 us
    dot_general x1, matrix products, shards(): jnp.einsum('spd,dtc->stpc', normed, value_split, preferred_element_type=j...  4.84 us
    another operation x1, local copies, waits for them, and re-layouts, shards(): own_keys = arrived[0].reshape(-1, local_heads, head_dim)  4.32 us
    slice x1, local copies, waits for them, and re-layouts, shards(): value_cache = arrived[1][None]  3.93 us
    reduce_sum x1, other arithmetic, shards(): jnp.mean(wide * wide, axis=-1, keepdims=True) + norm_epsilon  3.23 us
  transfers between devices with their start and end apart: 1, of which 1 were waited for; matrix products, arithmetic and copies ran while one was open for 0% of the time, Pallas kernels for 0%

profile of v1, /device:TPU:0, one launch (start us, length us, event | category | flops | bytes accessed | tf_op | source)
XLA Modules:
  0.0 157.8 jit_solution(10638655297935764112)
XLA Ops:
  0.7 3.2 %fusion = f32[8,128]{1,0:T(8,128)S(1)} fusion(bf16[8,128,2048]{2,1,0:T(8,128)(2,1)} %param.6), kind=kLoop, calls=%fused_computation.64 | loop fusion | flops 6290432 | bytes 4198400 | tf_op jit(solution)/shard_map/reduce_sum | solution.py:20
  4.1 7.2 %fusion.14 = bf16[8,128,4,256]{3,1,2,0:T(8,128)(2,1)S(1)} fusion(bf16[256,4,8,256]{3,2,1,0:T(8,128)(2,1)} %bitcast.278, bf16[8,128,2048]{2,1,0:T(8,128)(2,1)S(1)} %copy-done.2, f32[2048]{0:T(1024)S(1)} %convert_element_type.25, f32[8,128]{1,0:T(8,128)S(1)} %add_rsqrt_fusion), kind=kOutput, calls=%fused_computation.78 | convolution fusion | flops 4304404480 | bytes 10498048 | tf_op jit(solution)/shard_map/spd,dtc->stpc/dot_general | solution.py:25
  11.3 4.8 %fusion.17 = bf16[8,128,4,256]{3,1,2,0:T(8,128)(2,1)S(1)} fusion(bf16[256,4,8,256]{3,2,1,0:T(8,128)(2,1)S(1)} %bitcast.279, bf16[8,128,2048]{2,1,0:T(8,128)(2,1)S(1)} %copy-done.2, f32[2048]{0:T(1024)S(1)} %convert_element_type.25, f32[8,128]{1,0:T(8,128)S(1)} %add_rsqrt_fusion), kind=kOutput, calls=%fused_computation.79 | convolution fusion | flops 4304404480 | bytes 10498048 | tf_op jit(solution)/shard_map/spd,dtc->stpc/dot_general | solution.py:28
  17.5 0.7 bitcast_dynamic-update-slice_fusion.28
  18.1 0.7 bitcast_dynamic-update-slice_fusion.27
  18.8 0.7 bitcast_dynamic-update-slice_fusion.26
  19.5 0.7 bitcast_dynamic-update-slice_fusion.25
  20.1 0.7 bitcast_dynamic-update-slice_fusion.24
  20.8 0.7 bitcast_dynamic-update-slice_fusion.23
  22.1 0.7 bitcast_dynamic-update-slice_fusion.21
  22.8 0.7 bitcast_dynamic-update-slice_fusion.20
  23.4 0.7 bitcast_dynamic-update-slice_fusion.19
  24.1 0.7 bitcast_dynamic-update-slice_fusion.18
  24.8 0.7 bitcast_dynamic-update-slice_fusion.17
  25.4 0.7 bitcast_dynamic-update-slice_fusion.16
  26.1 0.7 bitcast_dynamic-update-slice_fusion.15
  27.4 0.7 bitcast_dynamic-update-slice_fusion.13
  28.0 0.7 bitcast_dynamic-update-slice_fusion.12
  28.7 0.7 bitcast_dynamic-update-slice_fusion.11
  30.0 0.7 bitcast_dynamic-update-slice_fusion.9
  31.3 0.7 bitcast_dynamic-update-slice_fusion.7
  32.0 0.7 bitcast_dynamic-update-slice_fusion.6
  35.3 0.7 bitcast_dynamic-update-slice_fusion.1
  36.6 0.7 fusion.52
  37.2 7.5 %all-to-all-start = ((bf16[32,1,2,128,256]{4,3,2,1,0:T(8,128)(2,1)}), bf16[32,1,2,128,256]{4,3,2,1,0:T(8,128)(2,1)}, u32[]{:S(2)}, u32[]{:S(2)}) async-start(bf16[32,1,2,128,256]{4,3,2,1,0:T(8,128)(2,1)} %fusion.52), calls=%async_computation | async-start | bytes 8388608 | tf_op jit(solution)/shard_map/all_to_all | solution.py:34
  44.8 94.1 %all-to-all-done = bf16[32,1,2,128,256]{4,3,2,1,0:T(8,128)(2,1)} async-done(((bf16[32,1,2,128,256]{4,3,2,1,0:T(8,128)(2,1)}), bf16[32,1,2,128,256]{4,3,2,1,0:T(8,128)(2,1)}, u32[]{:S(2)}, u32[]{:S(2)}) %all-to-all-start) | async-done | bytes 4194336 | tf_op jit(solution)/shard_map/all_to_all | solution.py:34
  139.0 3.9 %fusion.63 = (bf16[1,1,32,128,256]{4,3,1,0,2:T(8,128)(2,1)S(1)}, bf16[1,1,32,128,256]{4,3,1,0,2:T(8,128)(2,1)}) fusion(bf16[1,2,32,128,256]{4,3,1,0,2:T(8,128)(2,1)} %bitcast.41), kind=kLoop, calls=%fused_computation.166 | loop fusion | bytes 8388608 | tf_op jit(solution)/shard_map/slice | solution.py:41
  142.9 4.3 %reshape_squeeze.6 = bf16[4096,2,128]{2,1,0:T(2,128)(2,1)} reshape(bf16[1,1,32,128,256]{4,3,1,0,2:T(8,128)(2,1)} %get-tuple-element.4) | data formatting | bytes 4194304 | tf_op jit(solution)/shard_map/reshape;squeeze | solution.py:42
  147.2 2.2 %fusion.12 = f32[2,1,4096]{2,1,0:T(1,128)S(1)} fusion(bf16[4096,2,128]{2,1,0:T(2,128)(2,1)} %reshape_squeeze.6, bf16[1,256]{1,0:T(2,128)(2,1)S(1)} %copy-done), kind=kOutput, calls=%fused_computation.76 | convolution fusion | flops 2097152 | bytes 2130432 | tf_op jit(solution)/shard_map/hd,phd->hp/dot_general | solution.py:48
  149.6 2.5 %reduce-window.6 = f32[2,32,128]{2,1,0:T(8,128)S(1)} reduce-window(f32[2,32,128]{2,1,0:T(8,128)S(1)} %bitcast.274, f32[]{:T(128)} %constant.9.clone.1), window={size=1x1x128 pad=0_0x0_0x0_127}, to_apply=%region_1.2 | reduce-window | flops 1040384 | bytes 65540 | tf_op jit(solution)/shard_map/reduce-window
  152.9 2.1 %reshape_squeeze.7 = bf16[4096,2,128]{2,1,0:T(2,128)(2,1)} reshape(bf16[1,1,32,128,256]{4,3,1,0,2:T(8,128)(2,1)S(1)} %get-tuple-element.3) | data formatting | bytes 4194304 | tf_op jit(solution)/shard_map/reshape;squeeze | solution.py:43
  155.0 2.0 %fusion.10 = f32[2,1,128]{2,1,0:T(1,128)S(1)} fusion(bf16[4096,2,128]{2,1,0:T(2,128)(2,1)} %reshape_squeeze.7, bf16[2,4096,1]{1,0,2:T(2,128)(2,1)S(1)} %fusion.60), kind=kOutput, calls=%fused_computation.74 | convolution fusion | flops 2097152 | bytes 2114560 | tf_op jit(solution)/shard_map/hp,phd->hd/dot_general | solution.py:53
  (36 shorter events, 9.2 us)
Async XLA Ops:
  0.6 146.6 %copy-start = (bf16[1,256]{1,0:T(2,128)(2,1)S(1)}, bf16[1,256]{1,0:T(2,128)(2,1)}, u32[]{:S(2)}) copy-start(bf16[1,256]{1,0:T(2,128)(2,1)} %param.10) | copy-start | bytes 1540
  0.6 3.5 %copy-start.2 = (bf16[8,128,2048]{2,1,0:T(8,128)(2,1)S(1)}, bf16[8,128,2048]{2,1,0:T(8,128)(2,1)}, u32[]{:S(2)}) copy-start(bf16[8,128,2048]{2,1,0:T(8,128)(2,1)} %param.6) | copy-start | bytes 12582916
  0.7 3.3 %copy-start.3 = (bf16[2048]{0:T(1024)(128)(2,1)S(1)}, bf16[2048]{0:T(1024)(128)(2,1)}, u32[]{:S(2)}) copy-start(bf16[2048]{0:T(1024)(128)(2,1)} %param.7) | copy-start | bytes 12292
  4.1 7.2 %copy-start.4 = (bf16[2048,1024]{1,0:T(8,128)(2,1)S(1)}, bf16[2048,1024]{1,0:T(8,128)(2,1)}, u32[]{:S(2)}) copy-start(bf16[2048,1024]{1,0:T(8,128)(2,1)} %param.9) | copy-start | bytes 12582916
  37.2 7.5 %copy-start.5 = (f32[8]{0:T(128)S(1)}, f32[8]{0:T(128)}, u32[]{:S(2)}) copy-start(f32[8]{0:T(128)} %param.11) | copy-start | bytes 100
  37.2 101.7 %all-to-all-start = ((bf16[32,1,2,128,256]{4,3,2,1,0:T(8,128)(2,1)}), bf16[32,1,2,128,256]{4,3,2,1,0:T(8,128)(2,1)}, u32[]{:S(2)}, u32[]{:S(2)}) async-start(bf16[32,1,2,128,256]{4,3,2,1,0:T(8,128)(2,1)} %fusion.52), calls=%async_computation | async-start | bytes 8388608 | tf_op jit(solution)/shard_map/all_to_all | solution.py:34
  142.9 12.1 %copy-start.1 = (bf16[1,1,32,128,256]{4,3,1,0,2:T(8,128)(2,1)}, bf16[1,1,32,128,256]{4,3,1,0,2:T(8,128)(2,1)S(1)}, u32[]{:S(2)}) copy-start(bf16[1,1,32,128,256]{4,3,1,0,2:T(8,128)(2,1)S(1)} %get-tuple-element.3) | copy-start | bytes 6291460
